TPU v7x, 32 devices: a whole 2x2x4 slice. The times are simulated.
32 devices in a mesh: tp: 8 (over z, x), dp: 4 (over y, core).
Axes of the slice: x: 2, y: 2, z: 4, core: 2. Of those that a mesh axis runs over, the one named last changes fastest.
Arguments:
- tokens: bfloat16 [64, 4096], P(None, 'dp'), may hold values from -6 to 6
- recurrent_state: float32 [2, 64, 262144], P(None, 'dp', 'tp'), may hold values from -24 to 24
- pre_gain: float32 [2, 4096], P(None, 'dp'), may hold values from 0.1 to 1.9
- w_query: bfloat16 [2, 4096, 2048], P(None, 'dp', 'tp'), may hold values from -0.09375 to 0.09375
- w_key: bfloat16 [2, 4096, 2048], P(None, 'dp', 'tp'), may hold values from -0.09375 to 0.09375
- w_value: bfloat16 [2, 4096, 4096], P(None, 'dp', 'tp'), may hold values from -0.09375 to 0.09375
- w_gate: bfloat16 [2, 4096, 4096], P(None, 'dp', 'tp'), may hold values from -0.09375 to 0.09375
- w_decay: bfloat16 [2, 4096, 2048], P(None, 'dp', 'tp'), may hold values from -1 to 1
- decay_bias: float32 [2, 2048], P(None, 'tp'), may hold values from -5 to 3
- head_gain: float32 [2, 128], replicated, may hold values from 0.1 to 1.9
- w_out: bfloat16 [2, 4096, 4096], P(None, 'tp', 'dp'), may hold values from -0.09375 to 0.09375
- post_gain: float32 [2, 4096], P(None, 'dp'), may hold values from 0.1 to 1.9
Outputs:
- hidden_out: bfloat16 [64, 4096], P(None, 'dp')
- state_out: float32 [2, 64, 262144], P(None, 'dp', 'tp')
All inputs are finite; a program needn't handle non-finite values.
Results may differ from a plain program's by a relative error of at most 0.015.
Values may be sent and summed in bfloat16 or wider, within the bound.
A program may use at most 64 MiB of HBM per device.

v0:
```python
import jax
import jax.numpy as jnp
from jax import lax
from jax.sharding import PartitionSpec as P

D = 4096
KEY = 64
VAL = 128
epsilon = 1e-06


def local(
    tokens,
    recurrent_state,
    pre_gain,
    w_query,
    w_key,
    w_value,
    w_gate,
    w_decay,
    decay_bias,
    head_gain,
    w_out,
    post_gain,
):
    local_seqs = recurrent_state.shape[1]
    value_cols = recurrent_state.shape[2] // KEY
    heads_here = value_cols // VAL
    highest = lax.Precision.HIGHEST
    spread = (
        jnp.arange(value_cols, dtype=jnp.int32)[None, :] // VAL
        == jnp.arange(heads_here, dtype=jnp.int32)[:, None]
    ).astype(jnp.float32)

    def spread_heads(vectors):
        shaped = vectors.astype(jnp.float32).reshape(local_seqs, heads_here, KEY)
        return jnp.einsum("bhk,hc->bck", shaped, spread, precision=highest)

    residual = tokens
    new_states = []
    for section_index in range(2):
        wide_float = residual.astype(jnp.float32)
        squares_part = jnp.sum(wide_float * wide_float, axis=1)
        normed = (wide_float * pre_gain[section_index]).astype(jnp.bfloat16)
        partials = tuple(
            (
                jnp.dot(normed, weights[section_index], preferred_element_type=jnp.float32)
                for weights in (w_query, w_key, w_value, w_gate, w_decay)
            )
        )
        summed = lax.psum_scatter(partials + (squares_part,), "dp", scatter_dimension=0, tiled=True)
        projected = summed[:5]
        own_squares = summed[5]
        row_scale = lax.rsqrt(own_squares / D + epsilon)[:, None]
        query_part = (projected[0] * row_scale).astype(jnp.bfloat16)
        key_part = (projected[1] * row_scale).astype(jnp.bfloat16)
        values_own = projected[2] * row_scale
        gate_pre = projected[3] * row_scale
        log_decay = jax.nn.log_sigmoid(projected[4] * row_scale + decay_bias[section_index]) / 16.0
        query_cols = spread_heads(query_part)
        key_cols = spread_heads(key_part)
        decay_cols = jnp.exp(spread_heads(log_decay))
        old_state = recurrent_state[section_index].reshape(local_seqs, value_cols, KEY)
        new_state = decay_cols * old_state + key_cols * values_own[:, :, None]
        readout = jnp.sum(query_cols * new_state, axis=2) * KEY ** (-0.5)
        head_mean = jnp.mean(
            (readout * readout).reshape(local_seqs, heads_here, VAL), axis=2, keepdims=True
        )
        scaled = (
            readout.reshape(local_seqs, heads_here, VAL)
            * lax.rsqrt(head_mean + epsilon)
            * head_gain[section_index]
        )
        mixed = (scaled.reshape(local_seqs, value_cols) * jax.nn.silu(gate_pre)).astype(
            jnp.bfloat16
        )
        out_weight = w_out[section_index]
        partial_out = jnp.dot(
            lax.all_gather(mixed, "dp", axis=0, tiled=True),
            out_weight,
            preferred_element_type=jnp.float32,
        )
        out_rows = lax.psum(partial_out, "tp")
        out_squares = lax.psum(jnp.sum(out_rows * out_rows, axis=1), "dp")
        residual = (
            wide_float
            + out_rows * lax.rsqrt(out_squares / D + epsilon)[:, None] * post_gain[section_index]
        ).astype(jnp.bfloat16)
        new_states.append(new_state.reshape(local_seqs, value_cols * KEY))
    return (residual, jnp.stack(new_states))


def solution(mesh):
    in_specs = (
        P(None, "dp"),
        P(None, "dp", "tp"),
        P(None, "dp"),
        P(None, "dp", "tp"),
        P(None, "dp", "tp"),
        P(None, "dp", "tp"),
        P(None, "dp", "tp"),
        P(None, "dp", "tp"),
        P(None, "tp"),
        P(),
        P(None, "tp", "dp"),
        P(None, "dp"),
    )
    out_specs = (P(None, "dp"), P(None, "dp", "tp"))
    return jax.shard_map(local, mesh=mesh, in_specs=in_specs, out_specs=out_specs, check_vma=False)
```

profile of v0, /device:TPU:0, one launch (start us, length us, event | category | flops | bytes accessed | tf_op | source)
XLA Modules:
  0.0 412.4 jit_solution(11796743993679151280)
XLA Ops:
  7.2 0.9 fusion.85
  8.1 2.0 fusion.32
  10.1 1.9 fusion.30
  12.2 1.9 fusion.28
  14.2 0.9 fusion.14
  15.2 2.2 fusion.12
  17.6 3.9 fusion.83
  21.5 3.0 reshape_squeeze.6
  24.5 3.8 copy.18
  28.3 8.4 %all-reduce = f32[64]{0:T(128)S(1)} all-reduce(f32[64]{0:T(128)S(1)} %fusion.41), channel_id=3, replica_groups=mesh['tp'=8,'dp'=4] {'dp'}, use_global_device_ids=true, to_apply=%region_2.3.clone | all-reduce | flops 64 | bytes 512
  38.1 16.7 %reduce-scatter.13.cloned.1.call-done = f32[16,256]{1,0:T(8,128)} async-done(((f32[64,256]{1,0:T(8,128)}), f32[16,256]{1,0:T(8,128)}) %reduce-scatter.13.cloned.1.call-update) | async-done | bytes 16400 | tf_op jit(solution)/shard_map/reduce_scatter | solution.py:51
  54.7 22.0 %reduce-scatter.15.cloned.1.call-done = f32[16,256]{1,0:T(8,128)} async-done(((f32[64,256]{1,0:T(8,128)}), f32[16,256]{1,0:T(8,128)}) %reduce-scatter.15.cloned.1.call-update) | async-done | bytes 16400 | tf_op jit(solution)/shard_map/reduce_scatter | solution.py:51
  77.8 2.4 fusion.79
  80.2 19.1 %reduce-scatter.17.cloned.1.call-done = f32[16,512]{1,0:T(8,128)} async-done(((f32[64,512]{1,0:T(8,128)}), f32[16,512]{1,0:T(8,128)}) %reduce-scatter.17.cloned.1.call-update) | async-done | bytes 32784 | tf_op jit(solution)/shard_map/reduce_scatter | solution.py:51
  100.1 2.7 fusion.2
  103.5 17.7 %reduce-scatter.19.cloned.1.call-done = f32[16,512]{1,0:T(8,128)} async-done(((f32[64,512]{1,0:T(8,128)}), f32[16,512]{1,0:T(8,128)}) %reduce-scatter.19.cloned.1.call-update) | async-done | bytes 32784 | tf_op jit(solution)/shard_map/reduce_scatter | solution.py:51
  121.3 0.9 fusion.61
  122.2 5.2 %all_gather.6 = bf16[64,512]{1,0:T(8,128)(2,1)S(1)} all-gather(bf16[16,512]{1,0:T(8,128)(2,1)S(1)} %fusion.61), channel_id=1, replica_groups=mesh['tp'=8,'dp'=4] {'dp'}, dimensions={0}, use_global_device_ids=true | all-gather | bytes 81920 | tf_op jit(solution)/shard_map/all_gather | solution.py:79
  127.4 2.2 fusion.10
  129.7 4.2 %reshape_squeeze.7 = f32[16,512,64]{2,1,0:T(8,128)} reshape(f32[1,16,32768]{2,1,0:T(8,128)} %get-tuple-element.4) | data formatting | bytes 4194304 | tf_op jit(solution)/shard_map/reshape;squeeze | solution.py:63
  133.9 3.9 copy.19
  137.8 2.8 copy.20
  140.6 4.1 stack_reshape.6
  144.7 56.1 %all-reduce.5.cloned.1.call-done = f32[64,1024]{1,0:T(8,128)} async-done(((f32[64,1024]{1,0:T(8,128)}), f32[64,1024]{1,0:T(8,128)}) %all-reduce.5.cloned.1.call-update) | async-done | bytes 262160 | tf_op jit(solution)/shard_map/psum | solution.py:83
  200.8 1.1 multiply_reduce_fusion.1
  201.9 5.7 %psum.29 = f32[64]{0:T(128)S(1)} all-reduce(f32[64]{0:T(128)S(1)} %multiply_reduce_fusion.1), channel_id=1, replica_groups=mesh['tp'=8,'dp'=4] {'dp'}, use_global_device_ids=true, to_apply=%region_11.12 | all-reduce | flops 64 | bytes 512 | tf_op jit(solution)/shard_map/psum | solution.py:84
  207.5 1.2 fusion.44
  209.7 6.6 %all-reduce.1 = f32[64]{0:T(128)S(1)} all-reduce(f32[64]{0:T(128)S(1)} %get-tuple-element.2), channel_id=9, replica_groups=mesh['tp'=8,'dp'=4] {'dp'}, use_global_device_ids=true, to_apply=%region_14.15.clone | all-reduce | flops 64 | bytes 512
  217.2 1.9 fusion.22
  219.1 2.2 fusion.8
  221.5 2.2 fusion.6
  223.7 5.1 %reduce-scatter.21.cloned.1.call-done = f32[16,256]{1,0:T(8,128)} async-done(((f32[64,256]{1,0:T(8,128)}), f32[16,256]{1,0:T(8,128)}) %reduce-scatter.21.cloned.1.call-update) | async-done | bytes 16400 | tf_op jit(solution)/shard_map/reduce_scatter | solution.py:51
  228.8 22.0 %reduce-scatter.23.cloned.1.call-done = f32[16,256]{1,0:T(8,128)} async-done(((f32[64,256]{1,0:T(8,128)}), f32[16,256]{1,0:T(8,128)}) %reduce-scatter.23.cloned.1.call-update) | async-done | bytes 16400 | tf_op jit(solution)/shard_map/reduce_scatter | solution.py:51
  250.8 22.0 %reduce-scatter.25.cloned.1.call-done = f32[16,256]{1,0:T(8,128)} async-done(((f32[64,256]{1,0:T(8,128)}), f32[16,256]{1,0:T(8,128)}) %reduce-scatter.25.cloned.1.call-update) | async-done | bytes 16400 | tf_op jit(solution)/shard_map/reduce_scatter | solution.py:51
  273.7 2.4 fusion.75
  276.3 19.1 %reduce-scatter.27.cloned.1.call-done = f32[16,512]{1,0:T(8,128)} async-done(((f32[64,512]{1,0:T(8,128)}), f32[16,512]{1,0:T(8,128)}) %reduce-scatter.27.cloned.1.call-update) | async-done | bytes 32784 | tf_op jit(solution)/shard_map/reduce_scatter | solution.py:51
  296.2 2.8 fusion
  299.4 2.8 copy.21
  302.3 15.1 %reduce-scatter.29.cloned.1.call-done = f32[16,512]{1,0:T(8,128)} async-done(((f32[64,512]{1,0:T(8,128)}), f32[16,512]{1,0:T(8,128)}) %reduce-scatter.29.cloned.1.call-update) | async-done | bytes 32784 | tf_op jit(solution)/shard_map/reduce_scatter | solution.py:51
  317.5 0.9 fusion.58
  318.3 5.2 %all_gather.7 = bf16[64,512]{1,0:T(8,128)(2,1)S(1)} all-gather(bf16[16,512]{1,0:T(8,128)(2,1)S(1)} %fusion.58), channel_id=1, replica_groups=mesh['tp'=8,'dp'=4] {'dp'}, dimensions={0}, use_global_device_ids=true | all-gather | bytes 81920 | tf_op jit(solution)/shard_map/all_gather | solution.py:79
  323.6 2.2 fusion.4
  325.8 4.0 stack_reshape.7
  329.9 3.9 pad_maximum_fusion
  333.7 63.3 %all-reduce.7.cloned.1.call-done = f32[64,1024]{1,0:T(8,128)} async-done(((f32[64,1024]{1,0:T(8,128)}), f32[64,1024]{1,0:T(8,128)}) %all-reduce.7.cloned.1.call-update) | async-done | bytes 262160 | tf_op jit(solution)/shard_map/psum | solution.py:83
  397.1 1.1 multiply_reduce_fusion
  398.1 5.7 %psum.31 = f32[64]{0:T(128)S(1)} all-reduce(f32[64]{0:T(128)S(1)} %multiply_reduce_fusion), channel_id=1, replica_groups=mesh['tp'=8,'dp'=4] {'dp'}, use_global_device_ids=true, to_apply=%region_23.24 | all-reduce | flops 64 | bytes 512 | tf_op jit(solution)/shard_map/psum | solution.py:84
  403.8 1.7 fusion.45
  (79 shorter events, 8.6 us)
Async XLA Ops:
  7.2 7.0 %copy-start.1 = (bf16[64,1024]{1,0:T(8,128)(2,1)S(1)}, bf16[64,1024]{1,0:T(8,128)(2,1)}, u32[]{:S(2)}) copy-start(bf16[64,1024]{1,0:T(8,128)(2,1)} %param.12) | copy-start | bytes 393220
  7.2 7.0 %copy-start.5 = (bf16[2,1024,512]{2,1,0:T(8,128)(2,1)S(1)}, bf16[2,1024,512]{2,1,0:T(8,128)(2,1)}, u32[]{:S(2)}) copy-start(bf16[2,1024,512]{2,1,0:T(8,128)(2,1)} %param.17) | copy-start | bytes 6291460
  7.2 30.9 %reduce-scatter.11.cloned.1.call-start = ((), (), s32[]{:S(2)}) async-start(), calls=%async_computation.10 | async-start | bytes 81920 | tf_op jit(solution)/shard_map/reduce_scatter | solution.py:51
  10.1 44.6 %reduce-scatter.13.cloned.1.call-start = ((), (), s32[]{:S(2)}) async-start(), calls=%async_computation.11 | async-start | bytes 81920 | tf_op jit(solution)/shard_map/reduce_scatter | solution.py:51
  12.1 64.6 %reduce-scatter.15.cloned.1.call-start = ((), (), s32[]{:S(2)}) async-start(), calls=%async_computation.12 | async-start | bytes 81920 | tf_op jit(solution)/shard_map/reduce_scatter | solution.py:51
  14.1 85.1 %reduce-scatter.17.cloned.1.call-start = ((), (), s32[]{:S(2)}) async-start(), calls=%async_computation.13 | async-start | bytes 163840 | tf_op jit(solution)/shard_map/reduce_scatter | solution.py:51
  15.2 106.0 %reduce-scatter.19.cloned.1.call-start = ((), (), s32[]{:S(2)}) async-start(), calls=%async_computation.14 | async-start | bytes 163840 | tf_op jit(solution)/shard_map/reduce_scatter | solution.py:51
  17.4 183.4 %all-reduce.5.cloned.1.call-start = ((), (), s32[]{:S(2)}) async-start(), calls=%async_computation.15 | async-start | bytes 524288 | tf_op jit(solution)/shard_map/psum | solution.py:83
  24.5 12.2 %copy-start.3 = (f32[2,256]{1,0:T(2,128)S(1)}, f32[2,256]{1,0:T(2,128)}, u32[]{:S(2)}) copy-start(f32[2,256]{1,0:T(2,128)} %param.20) | copy-start | bytes 6148
  24.5 12.2 %copy-start.4 = (f32[2,128]{1,0:T(2,128)S(1)}, f32[2,128]{1,0:T(2,128)}, u32[]{:S(2)}) copy-start(f32[2,128]{1,0:T(2,128)} %param.21) | copy-start | bytes 3076
  24.5 12.3 %copy-start.8 = (u32[32]{0:T(128)S(1)}, u32[32]{0:T(128)}, u32[]{:S(2)}) copy-start(u32[32]{0:T(128)} %constant.51) | copy-start | bytes 388
  129.6 99.2 %reduce-scatter.21.cloned.1.call-start = ((), (), s32[]{:S(2)}) async-start(), calls=%async_computation.16 | async-start | bytes 81920 | tf_op jit(solution)/shard_map/reduce_scatter | solution.py:51
  133.9 3.9 copy-start.2
  140.6 68.1 %copy-start.6 = (bf16[2,1024,256]{2,1,0:T(8,128)(2,1)S(1)}, bf16[2,1024,256]{2,1,0:T(8,128)(2,1)}, u32[]{:S(2)}) copy-start(bf16[2,1024,256]{2,1,0:T(8,128)(2,1)} %param.15) | copy-start | bytes 3145732
  140.6 75.7 %copy-start.7 = (bf16[2,1024,256]{2,1,0:T(8,128)(2,1)S(1)}, bf16[2,1024,256]{2,1,0:T(8,128)(2,1)}, u32[]{:S(2)}) copy-start(bf16[2,1024,256]{2,1,0:T(8,128)(2,1)} %param.19) | copy-start | bytes 3145732
  209.6 41.2 %reduce-scatter.23.cloned.1.call-start = ((), (), s32[]{:S(2)}) async-start(), calls=%async_computation.17 | async-start | bytes 81920 | tf_op jit(solution)/shard_map/reduce_scatter | solution.py:51
  217.1 55.7 %reduce-scatter.25.cloned.1.call-start = ((), (), s32[]{:S(2)}) async-start(), calls=%async_computation.18 | async-start | bytes 81920 | tf_op jit(solution)/shard_map/reduce_scatter | solution.py:51
  219.1 76.2 %reduce-scatter.27.cloned.1.call-start = ((), (), s32[]{:S(2)}) async-start(), calls=%async_computation.19 | async-start | bytes 163840 | tf_op jit(solution)/shard_map/reduce_scatter | solution.py:51
  221.3 96.1 %reduce-scatter.29.cloned.1.call-start = ((), (), s32[]{:S(2)}) async-start(), calls=%async_computation.20 | async-start | bytes 163840 | tf_op jit(solution)/shard_map/reduce_scatter | solution.py:51
  223.6 173.4 %all-reduce.7.cloned.1.call-start = ((), (), s32[]{:S(2)}) async-start(), calls=%async_computation.21 | async-start | bytes 524288 | tf_op jit(solution)/shard_map/psum | solution.py:83
  325.8 4.0 copy-start
Sparse Core Ops, SparseCore 0:
  10.4 22.2 reduce-scatter.10
  35.1 19.5 reduce-scatter.12
  57.1 19.5 reduce-scatter.14
  79.6 19.6 reduce-scatter.16
  101.5 19.6 reduce-scatter.18
  129.8 70.9 all-reduce.4
  209.7 19.0 reduce-scatter.20
  231.2 19.5 reduce-scatter.22
  253.2 19.5 reduce-scatter.24
  275.6 19.6 reduce-scatter.26
  297.8 19.6 reduce-scatter.28
  326.0 71.0 all-reduce.6
where the time goes:
time: 414 us; the launch traced here: 412 us
  waiting for transfers between devices  278 us (67%)
  blocking collectives  36.8 us (9%)
  local copies, waits for them, and re-layouts  34.7 us (8%)
  matrix products  32.5 us (8%)
  between operations  15.1 us (4%)
  other arithmetic  14.5 us (4%)
    reduce_scatter x10, waiting for transfers between devices, local(): lax.psum_scatter(partials + (squares_part,), 'dp', scatter_dimension=0, t...  159 us
    psum x2, waiting for transfers between devices, local(): out_rows = lax.psum(partial_out, 'tp')  119 us
    dot_general x10, matrix products, local(): jnp.dot(normed, weights[section_index], preferred_element_type=jnp.float32)  16.9 us
    unnamed x2, blocking collectives  15 us
    another operation x4, local copies, waits for them, and re-layouts, local(): recurrent_state[section_index].reshape(local_seqs, value_cols, KEY)  14.9 us
    psum x2, blocking collectives, local(): out_squares = lax.psum(jnp.sum(out_rows * out_rows, axis=1), 'dp')  11.3 us
    dot_general x6, matrix products, spread_heads(): return jnp.einsum('bhk,hc->bck', shaped, spread, precision=highest)  11.2 us
    all_gather x2, blocking collectives, local(): lax.all_gather(mixed, 'dp', axis=0, tiled=True)  10.5 us
  transfers between devices with their start and end apart: 12, of which 11 were waited for; matrix products, arithmetic and copies ran while one was open for 16% of the time, Pallas kernels for 0%

commit v1 on v0

--- a/solution.py
+++ b/solution.py
@@ -80,7 +80,11 @@
             out_weight,
             preferred_element_type=jnp.float32,
         )
-        out_rows = lax.psum(partial_out, "tp")
+        out_rows = partial_out
+        for hop in (1, 2, 4):
+            out_rows = out_rows + lax.ppermute(
+                out_rows, "tp", [(dev, dev ^ hop) for dev in range(8)]
+            )
         out_squares = lax.psum(jnp.sum(out_rows * out_rows, axis=1), "dp")
         residual = (
             wide_float

time: 414 us -> 337 us (0.81)
  waiting for transfers between devices: 278 us -> 192 us
  starting transfers between devices: 0.5 us -> 11.5 us
    psum x2 -> x0, waiting for transfers between devices: 119 us -> none  [local(): out_rows = lax.psum(partial_out, 'tp')]
    ppermute x0 -> x6, waiting for transfers between devices: none -> 30.9 us  [local(): lax.ppermute(out_rows, 'tp', [(dev, dev ^ hop) for dev in range(8)])]
    ppermute x0 -> x6, starting transfers between devices: none -> 11.1 us  [local(): lax.ppermute(out_rows, 'tp', [(dev, dev ^ hop) for dev in range(8)])]
  transfers between devices with their start and end apart: 12 -> 16, of which waited for: 11 -> 14; matrix products, arithmetic and copies ran while one was open for 16% -> 20% of each run, Pallas kernels for 0% -> 0%
where the time goes in v1:
time: 337 us; the launch traced here: 336 us
  waiting for transfers between devices  192 us (57%)
  blocking collectives  36.6 us (11%)
  local copies, waits for them, and re-layouts  35.9 us (11%)
  matrix products  33.2 us (10%)
  between operations  15.1 us (4%)
  starting transfers between devices  11.5 us (3%)
  other arithmetic  10.8 us (3%)
    reduce_scatter x10, waiting for transfers between devices, local(): lax.psum_scatter(partials + (squares_part,), 'dp', scatter_dimension=0, t...  161 us
    ppermute x6, waiting for transfers between devices, local(): lax.ppermute(out_rows, 'tp', [(dev, dev ^ hop) for dev in range(8)])  30.9 us
    dot_general x10, matrix products, local(): jnp.dot(normed, weights[section_index], preferred_element_type=jnp.float32)  18.9 us
    another operation x4, local copies, waits for them, and re-layouts, local(): recurrent_state[section_index].reshape(local_seqs, value_cols, KEY)  14.9 us
    unnamed x2, blocking collectives  14.3 us
    psum x2, blocking collectives, local(): out_squares = lax.psum(jnp.sum(out_rows * out_rows, axis=1), 'dp')  11.6 us
    dot_general x6, matrix products, spread_heads(): return jnp.einsum('bhk,hc->bck', shaped, spread, precision=highest)  11.2 us
    ppermute x6, starting transfers between devices, local(): lax.ppermute(out_rows, 'tp', [(dev, dev ^ hop) for dev in range(8)])  11.1 us
  transfers between devices with their start and end apart: 16, of which 14 were waited for; matrix products, arithmetic and copies ran while one was open for 20% of the time, Pallas kernels for 0%

profile of v1, /device:TPU:0, one launch (start us, length us, event | category | flops | bytes accessed | tf_op | source)
XLA Modules:
  0.0 335.5 jit_solution(8048111818992998427)
XLA Ops:
  8.1 2.0 fusion.32
  10.1 1.9 fusion.30
  12.2 1.9 fusion.28
  15.2 2.2 fusion.12
  17.6 3.9 %fusion.83 = (f32[1,16,32768]{2,1,0:T(8,128)}, f32[1,16,32768]{2,1,0:T(8,128)S(1)}) fusion(f32[2,16,32768]{2,1,0:T(8,128)} %param.13), kind=kLoop, calls=%fused_computation.108 | loop fusion | bytes 8388608 | tf_op jit(solution)/shard_map/slice | solution.py:63
  21.5 3.0 reshape_squeeze.6
  24.5 3.8 %copy.18 = f32[16,512,64]{1,2,0:T(8,128)} copy(f32[16,512,64]{2,1,0:T(8,128)} %reshape_squeeze.6) | data formatting | bytes 4194304 | tf_op jit(solution)/shard_map/reshape;squeeze | solution.py:63
  28.3 8.4 %all-reduce = f32[64]{0:T(128)S(1)} all-reduce(f32[64]{0:T(128)S(1)} %fusion.41), channel_id=3, replica_groups=mesh['tp'=8,'dp'=4] {'dp'}, use_global_device_ids=true, to_apply=%region_2.3.clone | all-reduce | flops 64 | bytes 512
  38.1 16.7 %reduce-scatter.13.cloned.1.call-done = f32[16,256]{1,0:T(8,128)} async-done(((f32[64,256]{1,0:T(8,128)}), f32[16,256]{1,0:T(8,128)}) %reduce-scatter.13.cloned.1.call-update) | async-done | bytes 16400 | tf_op jit(solution)/shard_map/reduce_scatter | solution.py:51
  54.7 22.0 %reduce-scatter.15.cloned.1.call-done = f32[16,256]{1,0:T(8,128)} async-done(((f32[64,256]{1,0:T(8,128)}), f32[16,256]{1,0:T(8,128)}) %reduce-scatter.15.cloned.1.call-update) | async-done | bytes 16400 | tf_op jit(solution)/shard_map/reduce_scatter | solution.py:51
  77.8 2.4 fusion.79
  80.2 19.1 %reduce-scatter.17.cloned.1.call-done = f32[16,512]{1,0:T(8,128)} async-done(((f32[64,512]{1,0:T(8,128)}), f32[16,512]{1,0:T(8,128)}) %reduce-scatter.17.cloned.1.call-update) | async-done | bytes 32784 | tf_op jit(solution)/shard_map/reduce_scatter | solution.py:51
  100.1 2.8 fusion.2
  103.5 17.7 %reduce-scatter.19.cloned.1.call-done = f32[16,512]{1,0:T(8,128)} async-done(((f32[64,512]{1,0:T(8,128)}), f32[16,512]{1,0:T(8,128)}) %reduce-scatter.19.cloned.1.call-update) | async-done | bytes 32784 | tf_op jit(solution)/shard_map/reduce_scatter | solution.py:51
  122.1 5.2 %all_gather.6 = bf16[64,512]{1,0:T(8,128)(2,1)S(1)} all-gather(bf16[16,512]{1,0:T(8,128)(2,1)S(1)} %fusion.61), channel_id=1, replica_groups=mesh['tp'=8,'dp'=4] {'dp'}, dimensions={0}, use_global_device_ids=true | all-gather | bytes 81920 | tf_op jit(solution)/shard_map/all_gather | solution.py:79
  127.4 1.5 fusion.10
  130.4 7.1 %collective-permute-done = f32[64,1024]{1,0:T(8,128)S(1)} collective-permute-done((f32[64,1024]{1,0:T(8,128)S(1)}, f32[64,1024]{1,0:T(8,128)S(1)}, u32[]{:S(2)}, u32[]{:S(2)}) %collective-permute-start) | collective-permute-done | bytes 262176 | tf_op jit(solution)/shard_map/ppermute | solution.py:85
  137.5 1.5 collective-permute-start.1
  139.1 6.2 %collective-permute-done.1 = f32[64,1024]{1,0:T(8,128)S(1)} collective-permute-done((f32[64,1024]{1,0:T(8,128)S(1)}, f32[64,1024]{1,0:T(8,128)S(1)}, u32[]{:S(2)}, u32[]{:S(2)}) %collective-permute-start.1) | collective-permute-done | bytes 262176 | tf_op jit(solution)/shard_map/ppermute | solution.py:85
  145.4 2.4 collective-permute-start.2
  147.8 4.2 %reshape_squeeze.7 = f32[16,512,64]{2,1,0:T(8,128)} reshape(f32[1,16,32768]{2,1,0:T(8,128)} %get-tuple-element.8) | data formatting | bytes 4194304 | tf_op jit(solution)/shard_map/reshape;squeeze | solution.py:63
  152.0 3.9 %copy.19 = f32[16,512,64]{1,2,0:T(8,128)} copy(f32[16,512,64]{2,1,0:T(8,128)} %reshape_squeeze.7) | data formatting | bytes 4194304 | tf_op jit(solution)/shard_map/reshape;squeeze | solution.py:63
  155.9 2.9 collective-permute-done.2
  158.9 5.9 %psum.14 = f32[64]{0:T(128)S(1)} all-reduce(f32[64]{0:T(128)S(1)} %get-tuple-element.6), channel_id=1, replica_groups=mesh['tp'=8,'dp'=4] {'dp'}, use_global_device_ids=true, to_apply=%region_10.11 | all-reduce | flops 64 | bytes 512 | tf_op jit(solution)/shard_map/psum | solution.py:88
  165.0 1.9 fusion.26
  167.0 5.9 %all-reduce.1 = f32[64]{0:T(128)S(1)} all-reduce(f32[64]{0:T(128)S(1)} %get-tuple-element.4), channel_id=9, replica_groups=mesh['tp'=8,'dp'=4] {'dp'}, use_global_device_ids=true, to_apply=%region_13.14.clone | all-reduce | flops 64 | bytes 512
  172.9 1.9 fusion.24
  174.8 1.9 fusion.22
  176.8 2.2 fusion.8
  179.1 2.2 fusion.6
  181.3 6.3 %reduce-scatter.21.cloned.1.call-done = f32[16,256]{1,0:T(8,128)} async-done(((f32[64,256]{1,0:T(8,128)}), f32[16,256]{1,0:T(8,128)}) %reduce-scatter.21.cloned.1.call-update) | async-done | bytes 16400 | tf_op jit(solution)/shard_map/reduce_scatter | solution.py:51
  187.5 22.0 %reduce-scatter.23.cloned.1.call-done = f32[16,256]{1,0:T(8,128)} async-done(((f32[64,256]{1,0:T(8,128)}), f32[16,256]{1,0:T(8,128)}) %reduce-scatter.23.cloned.1.call-update) | async-done | bytes 16400 | tf_op jit(solution)/shard_map/reduce_scatter | solution.py:51
  209.6 22.0 %reduce-scatter.25.cloned.1.call-done = f32[16,256]{1,0:T(8,128)} async-done(((f32[64,256]{1,0:T(8,128)}), f32[16,256]{1,0:T(8,128)}) %reduce-scatter.25.cloned.1.call-update) | async-done | bytes 16400 | tf_op jit(solution)/shard_map/reduce_scatter | solution.py:51
  232.5 2.4 fusion.75
  235.1 19.3 %reduce-scatter.27.cloned.1.call-done = f32[16,512]{1,0:T(8,128)} async-done(((f32[64,512]{1,0:T(8,128)}), f32[16,512]{1,0:T(8,128)}) %reduce-scatter.27.cloned.1.call-update) | async-done | bytes 32784 | tf_op jit(solution)/shard_map/reduce_scatter | solution.py:51
  255.1 2.8 fusion
  259.9 16.4 %reduce-scatter.29.cloned.1.call-done = f32[16,512]{1,0:T(8,128)} async-done(((f32[64,512]{1,0:T(8,128)}), f32[16,512]{1,0:T(8,128)}) %reduce-scatter.29.cloned.1.call-update) | async-done | bytes 32784 | tf_op jit(solution)/shard_map/reduce_scatter | solution.py:51
  277.2 5.4 %all_gather.7 = bf16[64,512]{1,0:T(8,128)(2,1)S(1)} all-gather(bf16[16,512]{1,0:T(8,128)(2,1)S(1)} %fusion.58), channel_id=1, replica_groups=mesh['tp'=8,'dp'=4] {'dp'}, dimensions={0}, use_global_device_ids=true | all-gather | bytes 81920 | tf_op jit(solution)/shard_map/all_gather | solution.py:79
  285.7 7.1 %collective-permute-done.3 = f32[64,1024]{1,0:T(8,128)S(1)} collective-permute-done((f32[64,1024]{1,0:T(8,128)S(1)}, f32[64,1024]{1,0:T(8,128)S(1)}, u32[]{:S(2)}, u32[]{:S(2)}) %collective-permute-start.3) | collective-permute-done | bytes 262176 | tf_op jit(solution)/shard_map/ppermute | solution.py:85
  292.8 1.6 collective-permute-start.4
  294.4 2.8 copy.20
  297.1 4.0 %stack_reshape.6 = f32[1,16,32768]{2,1,0:T(8,128)} reshape(f32[16,512,64]{2,1,0:T(8,128)} %copy.20) | data formatting | bytes 4194304 | tf_op jit(solution)/shard_map/stack;reshape | solution.py:94
  301.1 2.8 copy.21
  303.9 4.1 %stack_reshape.7 = f32[1,16,32768]{2,1,0:T(8,128)} reshape(f32[16,512,64]{2,1,0:T(8,128)} %copy.21) | data formatting | bytes 4194304 | tf_op jit(solution)/shard_map/stack;reshape | solution.py:94
  308.0 2.5 collective-permute-start.5
  310.5 3.9 %pad_maximum_fusion = f32[2,16,32768]{2,1,0:T(8,128)} fusion(f32[1,16,32768]{2,1,0:T(8,128)} %stack_reshape.7, f32[1,16,32768]{2,1,0:T(8,128)S(1)} %copy-done.2), kind=kLoop, calls=%fused_computation | loop fusion | flops 1048576 | bytes 8388608 | tf_op jit(solution)/shard_map/stack | solution.py:94
  314.4 7.6 %collective-permute-done.5 = f32[64,1024]{1,0:T(8,128)S(1)} collective-permute-done((f32[64,1024]{1,0:T(8,128)S(1)}, f32[64,1024]{1,0:T(8,128)S(1)}, u32[]{:S(2)}, u32[]{:S(2)}) %collective-permute-start.5) | collective-permute-done | bytes 262176 | tf_op jit(solution)/shard_map/ppermute | solution.py:85
  322.1 5.8 %psum.15 = f32[64]{0:T(128)S(1)} all-reduce(f32[64]{0:T(128)S(1)} %get-tuple-element.2), channel_id=1, replica_groups=mesh['tp'=8,'dp'=4] {'dp'}, use_global_device_ids=true, to_apply=%region_21.22 | all-reduce | flops 64 | bytes 512 | tf_op jit(solution)/shard_map/psum | solution.py:88
  (89 shorter events, 17.6 us)
Async XLA Ops:
  7.2 7.0 %copy-start.3 = (bf16[64,1024]{1,0:T(8,128)(2,1)S(1)}, bf16[64,1024]{1,0:T(8,128)(2,1)}, u32[]{:S(2)}) copy-start(bf16[64,1024]{1,0:T(8,128)(2,1)} %param.12) | copy-start | bytes 393220
  7.2 7.0 %copy-start.7 = (bf16[2,1024,512]{2,1,0:T(8,128)(2,1)S(1)}, bf16[2,1024,512]{2,1,0:T(8,128)(2,1)}, u32[]{:S(2)}) copy-start(bf16[2,1024,512]{2,1,0:T(8,128)(2,1)} %param.17) | copy-start | bytes 6291460
  7.2 30.9 %reduce-scatter.11.cloned.1.call-start = ((), (), s32[]{:S(2)}) async-start(), calls=%async_computation.10 | async-start | bytes 81920 | tf_op jit(solution)/shard_map/reduce_scatter | solution.py:51
  10.1 44.6 %reduce-scatter.13.cloned.1.call-start = ((), (), s32[]{:S(2)}) async-start(), calls=%async_computation.11 | async-start | bytes 81920 | tf_op jit(solution)/shard_map/reduce_scatter | solution.py:51
  12.1 64.6 %reduce-scatter.15.cloned.1.call-start = ((), (), s32[]{:S(2)}) async-start(), calls=%async_computation.12 | async-start | bytes 81920 | tf_op jit(solution)/shard_map/reduce_scatter | solution.py:51
  14.1 85.1 %reduce-scatter.17.cloned.1.call-start = ((), (), s32[]{:S(2)}) async-start(), calls=%async_computation.13 | async-start | bytes 163840 | tf_op jit(solution)/shard_map/reduce_scatter | solution.py:51
  15.2 106.0 %reduce-scatter.19.cloned.1.call-start = ((), (), s32[]{:S(2)}) async-start(), calls=%async_computation.14 | async-start | bytes 163840 | tf_op jit(solution)/shard_map/reduce_scatter | solution.py:51
  17.4 170.1 %reduce-scatter.21.cloned.1.call-start = ((), (), s32[]{:S(2)}) async-start(), calls=%async_computation.15 | async-start | bytes 81920 | tf_op jit(solution)/shard_map/reduce_scatter | solution.py:51
  24.5 12.2 %copy-start.5 = (f32[2,256]{1,0:T(2,128)S(1)}, f32[2,256]{1,0:T(2,128)}, u32[]{:S(2)}) copy-start(f32[2,256]{1,0:T(2,128)} %param.20) | copy-start | bytes 6148
  24.5 12.2 %copy-start.6 = (f32[2,128]{1,0:T(2,128)S(1)}, f32[2,128]{1,0:T(2,128)}, u32[]{:S(2)}) copy-start(f32[2,128]{1,0:T(2,128)} %param.21) | copy-start | bytes 3076
  24.5 12.3 %copy-start.8 = (u32[32]{0:T(128)S(1)}, u32[32]{0:T(128)}, u32[]{:S(2)}) copy-start(u32[32]{0:T(128)} %constant.51) | copy-start | bytes 388
  128.9 8.6 %collective-permute-start = (f32[64,1024]{1,0:T(8,128)S(1)}, f32[64,1024]{1,0:T(8,128)S(1)}, u32[]{:S(2)}, u32[]{:S(2)}) collective-permute-start(f32[64,1024]{1,0:T(8,128)S(1)} %fusion.10), channel_id=1, source_target_pairs={{0,4},{4,0},{8,12},{12,8},{16,20},{20,16},{24,28},{28,24},{1,5},{5... | collective-permute-start | bytes 786440 | tf_op jit(solution)/shard_map/ppermute | solution.py:85
  137.5 7.8 %collective-permute-start.1 = (f32[64,1024]{1,0:T(8,128)S(1)}, f32[64,1024]{1,0:T(8,128)S(1)}, u32[]{:S(2)}, u32[]{:S(2)}) collective-permute-start(f32[64,1024]{1,0:T(8,128)S(1)} %add.135), channel_id=1, source_target_pairs={{0,8},{4,12},{8,0},{12,4},{16,24},{20,28},{24,16},{28,20},{1,9},{5... | collective-permute-start | bytes 786440 | tf_op jit(solution)/shard_map/ppermute | solution.py:85
  145.4 13.4 %collective-permute-start.2 = (f32[64,1024]{1,0:T(8,128)S(1)}, f32[64,1024]{1,0:T(8,128)S(1)}, u32[]{:S(2)}, u32[]{:S(2)}) collective-permute-start(f32[64,1024]{1,0:T(8,128)S(1)} %add.136), channel_id=1, source_target_pairs={{0,16},{4,20},{8,24},{12,28},{16,0},{20,4},{24,8},{28,12},{1,17},{... | collective-permute-start | bytes 786440 | tf_op jit(solution)/shard_map/ppermute | solution.py:85
  152.0 3.9 %copy-start.4 = (f32[2,1024]{1,0:T(2,128)S(1)}, f32[2,1024]{1,0:T(2,128)}, u32[]{:S(2)}) copy-start(f32[2,1024]{1,0:T(2,128)} %param.23) | copy-start | bytes 24580
  166.9 42.6 %reduce-scatter.23.cloned.1.call-start = ((), (), s32[]{:S(2)}) async-start(), calls=%async_computation.16 | async-start | bytes 81920 | tf_op jit(solution)/shard_map/reduce_scatter | solution.py:51
  174.8 56.8 %reduce-scatter.25.cloned.1.call-start = ((), (), s32[]{:S(2)}) async-start(), calls=%async_computation.17 | async-start | bytes 81920 | tf_op jit(solution)/shard_map/reduce_scatter | solution.py:51
  176.7 77.6 %reduce-scatter.27.cloned.1.call-start = ((), (), s32[]{:S(2)}) async-start(), calls=%async_computation.18 | async-start | bytes 163840 | tf_op jit(solution)/shard_map/reduce_scatter | solution.py:51
  179.0 97.3 %reduce-scatter.29.cloned.1.call-start = ((), (), s32[]{:S(2)}) async-start(), calls=%async_computation.19 | async-start | bytes 163840 | tf_op jit(solution)/shard_map/reduce_scatter | solution.py:51
  257.9 1.4 copy-start
  284.1 8.6 %collective-permute-start.3 = (f32[64,1024]{1,0:T(8,128)S(1)}, f32[64,1024]{1,0:T(8,128)S(1)}, u32[]{:S(2)}, u32[]{:S(2)}) collective-permute-start(f32[64,1024]{1,0:T(8,128)S(1)} %fusion.4), channel_id=1, source_target_pairs={{0,4},{4,0},{8,12},{12,8},{16,20},{20,16},{24,28},{28,24},{1,5},{5... | collective-permute-start | bytes 786440 | tf_op jit(solution)/shard_map/ppermute | solution.py:85
  292.8 15.2 %collective-permute-start.4 = (f32[64,1024]{1,0:T(8,128)S(1)}, f32[64,1024]{1,0:T(8,128)S(1)}, u32[]{:S(2)}, u32[]{:S(2)}) collective-permute-start(f32[64,1024]{1,0:T(8,128)S(1)} %add.148), channel_id=1, source_target_pairs={{0,8},{4,12},{8,0},{12,4},{16,24},{20,28},{24,16},{28,20},{1,9},{5... | collective-permute-start | bytes 786440 | tf_op jit(solution)/shard_map/ppermute | solution.py:85
  297.1 4.0 %copy-start.1 = (f32[16,512,64]{1,2,0:T(8,128)S(1)}, f32[16,512,64]{1,2,0:T(8,128)}, u32[]{:S(2)}) copy-start(f32[16,512,64]{1,2,0:T(8,128)} %copy-done) | copy-start | bytes 6291460
  303.9 6.6 %copy-start.2 = (f32[1,16,32768]{2,1,0:T(8,128)S(1)}, f32[1,16,32768]{2,1,0:T(8,128)}, u32[]{:S(2)}) copy-start(f32[1,16,32768]{2,1,0:T(8,128)} %stack_reshape.6) | copy-start | bytes 6291460
  308.0 14.0 %collective-permute-start.5 = (f32[64,1024]{1,0:T(8,128)S(1)}, f32[64,1024]{1,0:T(8,128)S(1)}, u32[]{:S(2)}, u32[]{:S(2)}) collective-permute-start(f32[64,1024]{1,0:T(8,128)S(1)} %add.149), channel_id=1, source_target_pairs={{0,16},{4,20},{8,24},{12,28},{16,0},{20,4},{24,8},{28,12},{1,17},{... | collective-permute-start | bytes 786440 | tf_op jit(solution)/shard_map/ppermute | solution.py:85
Sparse Core Ops, SparseCore 0:
  10.4 22.2 reduce-scatter.10
  35.1 19.5 reduce-scatter.12
  57.1 19.5 reduce-scatter.14
  79.6 19.6 reduce-scatter.16
  101.5 19.6 reduce-scatter.18
  167.1 20.4 reduce-scatter.20
  190.0 19.5 reduce-scatter.22
  212.0 19.5 reduce-scatter.24
  234.6 19.6 reduce-scatter.26
  256.6 19.6 reduce-scatter.28
